TPU v7x, 32 devices: a whole 2x2x4 slice. The times are simulated.
32 devices in a mesh: sp: 16 (over z, y, core), tp: 2 (over x).
Axes of the slice: x: 2, y: 2, z: 4, core: 2. Of those that a mesh axis runs over, the one named last changes fastest.
Arguments:
- tokens: bfloat16 [4096, 2048], P(('sp', 'tp')), may hold values from -6 to 6
- norm_gain: float32 [2048], replicated, may hold values from 0.1 to 1.9
- w_query: bfloat16 [2048, 1024], P('sp', 'tp'), may hold values from -0.125 to 0.125
- w_forget: bfloat16 [2048, 1024], P('sp', 'tp'), may hold values from -0.125 to 0.125
- w_input: bfloat16 [2048, 1024], P('sp', 'tp'), may hold values from -0.125 to 0.125
- w_outgate: bfloat16 [2048, 1024], P('sp', 'tp'), may hold values from -0.125 to 0.125
- w_bgate: bfloat16 [2048, 1024], P('sp', 'tp'), may hold values from -0.125 to 0.125
- w_cgate: bfloat16 [2048, 1024], P('sp', 'tp'), may hold values from -0.125 to 0.125
- w_value: bfloat16 [2048, 1024], P('sp', 'tp'), may hold values from -0.125 to 0.125
- floor_gap: float32 [8, 128], P('tp'), may hold values from 0 to 0.06
- extra_decay: float32 [4096, 8], P('sp', 'tp'), may hold values from -1 to 0
- start_state: float32 [8, 128, 128], P('tp'), may hold values from -0.109375 to 0.109375
- state_gain: float32 [128], replicated, may hold values from 0.1 to 1.9
- conv_taps: float32 [3, 1024], P(None, 'tp'), may hold values from -3 to 3
- out_rec: bfloat16 [1024, 2048], P('tp', 'sp'), may hold values from -0.125 to 0.125
- out_conv: bfloat16 [1024, 2048], P('tp', 'sp'), may hold values from -0.125 to 0.125
Outputs:
- mixed_sum: bfloat16 [4096, 2048], P(('sp', 'tp'))
All inputs are finite; a program needn't handle non-finite values.
Results may differ from a plain program's by a relative error of at most 0.018.
Values may be sent and summed in bfloat16 or wider, within the bound.
A program may use at most 64 MiB of HBM per device.

v0:
```python
import jax
import jax.numpy as jnp
from jax import lax
from jax.sharding import PartitionSpec as P

BLOCK = 64


eps = 1e-06
highest_precision = lax.Precision.HIGHEST


def prefix(value, axis, join, neutral):
    count, mine = (lax.axis_size(axis), lax.axis_index(axis))
    pieces = jax.tree.map(lambda part: lax.all_gather(part, axis), value)
    so_far = jax.tree.map(
        lambda part, zero: jnp.full_like(part, 0) + jnp.asarray(zero, part.dtype), value, neutral
    )

    def hop(position, so_far):
        longer = join(so_far, jax.tree.map(lambda part: part[position], pieces))
        return jax.tree.map(lambda new, old: jnp.where(position < mine, new, old), longer, so_far)

    return lax.fori_loop(0, count - 1, hop, so_far)


def shifted(block, axis, distance):
    devices = range(lax.axis_size(axis))
    route = [(i - distance, i) for i in devices if i - distance in devices]
    return lax.ppermute(block, axis, route)


def rms_scale(values):
    return lax.rsqrt(jnp.mean(values * values, axis=-1, keepdims=True) + eps)


def local_blocks(queries, write_in, inputs, log_keep, block_len):
    length, head_count, address_feature_count = queries.shape
    value_dim = inputs.shape[-1]
    blocks_count = length // block_len

    def blocked(tensor):
        return tensor.reshape(blocks_count, block_len, head_count, tensor.shape[-1]).transpose(
            0, 2, 1, 3
        )

    def unblock(tensor):
        return tensor.transpose(0, 2, 1, 3).reshape(length, head_count, tensor.shape[-1])

    causal = (jnp.arange(block_len)[:, None] >= jnp.arange(block_len)[None, :])[None, :, :, None]

    def advance(carried, pieces):
        memory_state, offset = carried
        query_block, write_blk, input_block, keep_blk = pieces
        running_state = jnp.cumsum(keep_blk, axis=1)
        spread = running_state[:, :, None, :] - running_state[:, None, :, :]
        decays = jnp.where(causal, jnp.exp(jnp.minimum(spread, 0.0)), 0.0)
        scores = jnp.sum(query_block[:, :, None, :] * write_blk[:, None, :, :] * decays, axis=-1)
        final_output = jnp.einsum(
            "qcp,qpi->qci",
            query_block * jnp.exp(running_state),
            memory_state,
            precision=highest_precision,
        )
        final_output = final_output + jnp.einsum(
            "hts,hsv->htv", scores, input_block, precision=highest_precision
        )
        lifted_state = query_block * jnp.exp(running_state + offset[:, None, :])
        final_state = running_state[:, -1, :]
        weighted_value = write_blk * jnp.exp(final_state[:, None, :] - running_state)
        memory_state = memory_state * jnp.exp(final_state)[:, :, None] + jnp.einsum(
            "euz,eul->ezl", weighted_value, input_block, precision=highest_precision
        )
        return ((memory_state, offset + final_state), (final_output, lifted_state))

    initial = (
        jnp.zeros((head_count, address_feature_count, value_dim), jnp.float32),
        jnp.zeros((head_count, address_feature_count), jnp.float32),
    )
    finals, outputs = lax.scan(
        advance, initial, (blocked(queries), blocked(write_in), blocked(inputs), blocked(log_keep))
    )
    return (unblock(outputs[0]), unblock(outputs[1]), finals[0], jnp.exp(finals[1]))


def chain(earlier, later):
    return (earlier[0] * later[0], earlier[1] * later[0][:, :, None] + later[1])


def on_device(
    tokens,
    norm_gain,
    w_query,
    w_forget,
    w_input,
    w_outgate,
    w_bgate,
    w_cgate,
    w_value,
    floor_gap,
    extra_decay,
    start_state,
    state_gain,
    conv_taps,
    out_rec,
    out_conv,
):
    tokens_f = tokens.astype(jnp.float32)
    normed = (tokens_f * rms_scale(tokens_f) * norm_gain).astype(jnp.bfloat16)
    weights = (w_query, w_forget, w_input, w_outgate, w_bgate, w_cgate, w_value)
    whole_weights = (
        lax.all_gather(w_query, "sp", axis=0, tiled=True),
        lax.all_gather(w_forget, "sp", axis=0, tiled=True),
        lax.all_gather(w_input, "sp", axis=0, tiled=True),
        lax.all_gather(w_outgate, "sp", axis=0, tiled=True),
        lax.all_gather(w_bgate, "sp", axis=0, tiled=True),
        lax.all_gather(w_cgate, "sp", axis=0, tiled=True),
        lax.all_gather(w_value, "sp", axis=0, tiled=True),
    )

    def project(shard_rows):
        return jnp.concatenate(
            [
                jnp.dot(shard_rows, matrix, preferred_element_type=jnp.float32).astype(jnp.bfloat16)
                for matrix in whole_weights
            ],
            axis=1,
        )

    joined = project(lax.all_gather(normed, "tp", axis=0, tiled=True))
    borders = [0]
    for matrix in weights:
        borders.append(borders[-1] + matrix.shape[1])
    projected = [joined[:, borders[number] : borders[number + 1]] for number in range(len(weights))]
    query_raw, forget_raw, input_raw, outgate_raw, bgate_raw, cgate_raw, value_raw = projected
    length = query_raw.shape[0]
    head_count, address_feature_count = floor_gap.shape
    value_dim = start_state.shape[2]
    queries = jax.nn.silu(query_raw.astype(jnp.float32)).reshape(
        length, head_count, address_feature_count
    )
    write_in = floor_gap[None] * jax.nn.sigmoid(-forget_raw.astype(jnp.float32)).reshape(
        length, head_count, address_feature_count
    )
    log_keep = jnp.log1p(-write_in) + extra_decay[:, :, None]
    inputs = input_raw.astype(jnp.float32).reshape(length, head_count, value_dim)
    output_list, lifted_state, memory_state, kept = local_blocks(
        queries, write_in, inputs, log_keep, BLOCK
    )
    before_keep, before_memory = prefix(
        (kept, memory_state), "sp", chain, (jnp.ones_like(kept), jnp.zeros_like(memory_state))
    )
    carried_hidden_prior = start_state * before_keep[:, :, None] + before_memory
    blended_state = output_list + jnp.einsum(
        "sqa,qar->sqr", lifted_state, carried_hidden_prior, precision=highest_precision
    )
    gate_out = jax.nn.silu(outgate_raw.astype(jnp.float32)).reshape(length, head_count, value_dim)
    rec_out = (
        (blended_state * rms_scale(blended_state) * state_gain * gate_out)
        .reshape(length, head_count * value_dim)
        .astype(jnp.bfloat16)
    )
    rim_rows = jnp.stack([cgate_raw[length - 2 :], value_raw[length - 2 :]])
    before_rim = shifted(rim_rows, "sp", 1)
    convolution_gate_widened = jnp.concatenate([before_rim[0], cgate_raw], axis=0).astype(
        jnp.float32
    )
    value_ext = jnp.concatenate([before_rim[1], value_raw], axis=0).astype(jnp.float32)
    gated = convolution_gate_widened * value_ext
    conv_out = (
        conv_taps[0] * gated[:length]
        + conv_taps[1] * gated[1 : length + 1]
        + conv_taps[2] * gated[2:]
    )
    short_out = (bgate_raw.astype(jnp.float32) * conv_out).astype(jnp.bfloat16)
    rec_weight, conv_weight = (
        lax.all_gather(out_rec, "sp", axis=1, tiled=True),
        lax.all_gather(out_conv, "sp", axis=1, tiled=True),
    )
    product = jnp.dot(rec_out, rec_weight, preferred_element_type=jnp.float32)
    return lax.psum_scatter(
        (product + jnp.dot(short_out, conv_weight, preferred_element_type=jnp.float32)).astype(
            jnp.bfloat16
        ),
        "tp",
        scatter_dimension=0,
        tiled=True,
    )


def solution(mesh):
    placed = (
        P(("sp", "tp"), None),
        P(),
        P("sp", "tp"),
        P("sp", "tp"),
        P("sp", "tp"),
        P("sp", "tp"),
        P("sp", "tp"),
        P("sp", "tp"),
        P("sp", "tp"),
        P("tp", None),
        P("sp", "tp"),
        P("tp", None, None),
        P(),
        P(None, "tp"),
        P("tp", "sp"),
        P("tp", "sp"),
    )
    return jax.shard_map(
        on_device, mesh=mesh, in_specs=placed, out_specs=P(("sp", "tp"), None), check_vma=False
    )
```

profile of v0, /device:TPU:24, one launch (start us, length us, event | category | flops | bytes accessed | tf_op | source)
XLA Modules:
  0.0 496.4 jit_solution(12257426766689084749)
XLA Ops:
  6.5 1.2 fusion.37
  7.8 2.0 fusion.39
  9.9 0.7 all-gather.19.cloned.1.call-update
  10.6 0.7 all-gather.21.cloned.1.call-update
  13.1 0.7 all-gather.23.cloned.1.call-update
  14.0 18.2 %all-gather.15.cloned.1.call-done = bf16[256,2048]{1,0:T(8,128)(2,1)} async-done(((bf16[128,2048]{1,0:T(8,128)(2,1)}), bf16[256,2048]{1,0:T(8,128)(2,1)}) %all-gather.15.cloned.1.call-update) | async-done | bytes 1048592 | tf_op jit(solution)/shard_map/all_gather | solution.py:130
  32.3 42.4 %all-gather.19.cloned.1.call-done = bf16[2048,512]{1,0:T(8,128)(2,1)} async-done(((bf16[128,512]{1,0:T(8,128)(2,1)}), bf16[2048,512]{1,0:T(8,128)(2,1)}) %all-gather.19.cloned.1.call-update) | async-done | bytes 2097168 | tf_op jit(solution)/shard_map/all_gather | solution.py:114
  74.6 2.6 fusion.31
  77.4 39.6 %all-gather.21.cloned.1.call-done = bf16[2048,512]{1,0:T(8,128)(2,1)} async-done(((bf16[128,512]{1,0:T(8,128)(2,1)}), bf16[2048,512]{1,0:T(8,128)(2,1)}) %all-gather.21.cloned.1.call-update) | async-done | bytes 2097168 | tf_op jit(solution)/shard_map/all_gather | solution.py:112
  117.0 2.4 divide_multiply_fusion.1
  119.6 39.7 %all-gather.17.cloned.1.call-done = bf16[2048,512]{1,0:T(8,128)(2,1)} async-done(((bf16[128,512]{1,0:T(8,128)(2,1)}), bf16[2048,512]{1,0:T(8,128)(2,1)}) %all-gather.17.cloned.1.call-update) | async-done | bytes 2097168 | tf_op jit(solution)/shard_map/all_gather | solution.py:113
  159.2 3.2 fusion.30
  162.4 1.2 reshape.81
  164.0 22.6 %while.33 = (s32[]{:T(128)}, f32[4,128,128]{2,1,0:T(8,128)S(1)}, f32[4,128]{1,0:T(4,128)S(1)}, f32[4,4,64,128]{3,2,0,1:T(8,128)}, f32[4,4,64,128]{3,2,0,1:T(8,12...) while((s32[]{:T(128)}, f32[4,128,128]{2,1,0:T(8,128)S(1)}, ...), condition=%wide.region_4.5_spmd.clone, body=%wide.region_1.4_spmd.clone.sunk | while | flops 140923904 | bytes 4028565 | solution.py:80
  164.2 3.4 multiply_reduce_fusion.3
  167.9 1.0 fusion.93
  169.0 0.7 convolution_add_fusion.4
  169.9 3.4 multiply_reduce_fusion.3
  173.6 1.0 fusion.93
  174.6 0.7 convolution_add_fusion.4
  175.5 3.4 multiply_reduce_fusion.3
  179.2 1.0 fusion.93
  180.3 0.7 convolution_add_fusion.4
  181.2 3.4 multiply_reduce_fusion.3
  184.9 1.0 fusion.93
  185.9 0.7 convolution_add_fusion.4
  186.6 0.7 copy-done
  187.4 0.7 all-gather.25.cloned.1.call-update
  188.2 0.5 all-gather.27.cloned.1.call-update
  188.7 0.7 all-gather.33.cloned.1.call-update
  189.5 11.9 %all-gather.31.cloned.1.call-done = bf16[2048,512]{1,0:T(8,128)(2,1)} async-done(((bf16[128,512]{1,0:T(8,128)(2,1)}), bf16[2048,512]{1,0:T(8,128)(2,1)}) %all-gather.31.cloned.1.call-update) | async-done | bytes 2097168 | tf_op jit(solution)/shard_map/all_gather | solution.py:118
  201.4 2.6 convolution_convert_fusion
  204.1 39.6 %all-gather.29.cloned.1.call-done = bf16[2048,512]{1,0:T(8,128)(2,1)} async-done(((bf16[128,512]{1,0:T(8,128)(2,1)}), bf16[2048,512]{1,0:T(8,128)(2,1)}) %all-gather.29.cloned.1.call-update) | async-done | bytes 2097168 | tf_op jit(solution)/shard_map/all_gather | solution.py:117
  243.7 2.3 convolution_convert_fusion.1
  246.0 2.3 collective-permute-start
  248.3 37.7 %all-gather.23.cloned.1.call-done = bf16[2048,512]{1,0:T(8,128)(2,1)} async-done(((bf16[128,512]{1,0:T(8,128)(2,1)}), bf16[2048,512]{1,0:T(8,128)(2,1)}) %all-gather.23.cloned.1.call-update) | async-done | bytes 2097168 | tf_op jit(solution)/shard_map/all_gather | solution.py:115
  286.0 3.2 divide_multiply_fusion
  289.2 16.1 %all-gather.2 = f32[16,4,128]{2,1,0:T(4,128)S(1)} all-gather(f32[1,4,128]{2,1,0:T(4,128)S(1)} %exponential_bitcast_fusion), channel_id=2, replica_groups=mesh['sp'=16,'tp'=2] {'sp'}, dimensions={0}, use_global_device_ids=true | all-gather | bytes 34816 | tf_op jit(solution)/shard_map/all_gather | solution.py:15
  305.5 1.2 copy.52
  306.8 1.1 convert_multiply_fusion.2
  307.9 29.4 %all-gather.35.cloned.1.call-done = f32[64,128,128]{2,1,0:T(8,128)} async-done(((f32[4,128,128]{2,1,0:T(8,128)}), f32[64,128,128]{2,1,0:T(8,128)}) %all-gather.35.cloned.1.call-update) | async-done | bytes 4194320 | tf_op jit(solution)/shard_map/all_gather | solution.py:15
  337.2 18.0 %while.34 = (s32[]{:T(128)}, f32[4,128]{1,0:T(4,128)S(1)}, f32[4,128,128]{2,1,0:T(8,128)S(1)}, s32[]{:T(128)}, f32[16,4,128]{2,1,0:T(4,128)S(1)}, /*index=5*/f32[16,4,128,128]{3,2,1,0:T(8,128)}, s32[]{:T(128)}, s32[]{:T(128)}) while((s32[]{:T(128)}, f32[4,128]{1,0:T(4,128)S(1)}, f32[4,128,128]{2,1,0:T(8,128)S(1)}, s32[]{:T(128)}, ...), condition=%wide.region_6.7_spmd.clone, body=%wide.region_5.6_spmd.clone.sunk | while | flops 263684 | bytes 796787 | solution.py:24
  337.2 1.1 fusion.94
  338.4 1.2 fusion.94
  339.6 1.2 fusion.94
  340.8 1.2 fusion.94
  342.0 1.2 fusion.94
  343.2 1.2 fusion.94
  344.4 1.2 fusion.94
  345.6 1.2 fusion.94
  346.8 1.2 fusion.94
  348.0 1.2 fusion.94
  349.2 1.2 fusion.94
  350.4 1.2 fusion.94
  351.6 1.2 fusion.94
  352.8 1.2 fusion.94
  354.0 1.2 fusion.94
  355.2 0.7 multiply_reduce_fusion.1
  356.1 22.8 %all-gather.25.cloned.1.call-done = bf16[512,2048]{1,0:T(8,128)(2,1)} async-done(((bf16[512,128]{1,0:T(8,128)(2,1)}), bf16[512,2048]{1,0:T(8,128)(2,1)}) %all-gather.25.cloned.1.call-update) | async-done | bytes 2097168 | tf_op jit(solution)/shard_map/all_gather | solution.py:177
  378.9 2.3 fusion.53
  381.2 40.5 %all-gather.27.cloned.1.call-done = bf16[2048,512]{1,0:T(8,128)(2,1)} async-done(((bf16[128,512]{1,0:T(8,128)(2,1)}), bf16[2048,512]{1,0:T(8,128)(2,1)}) %all-gather.27.cloned.1.call-update) | async-done | bytes 2097168 | tf_op jit(solution)/shard_map/all_gather | solution.py:116
  421.8 41.7 %all-gather.33.cloned.1.call-done = bf16[512,2048]{1,0:T(8,128)(2,1)} async-done(((bf16[512,128]{1,0:T(8,128)(2,1)}), bf16[512,2048]{1,0:T(8,128)(2,1)}) %all-gather.33.cloned.1.call-update) | async-done | bytes 2097168 | tf_op jit(solution)/shard_map/all_gather | solution.py:178
  463.4 4.9 fusion.25
  468.4 21.2 %reduce-scatter.2.cloned.1.call-done = bf16[128,2048]{1,0:T(8,128)(2,1)} async-done(((bf16[256,2048]{1,0:T(8,128)(2,1)}), bf16[128,2048]{1,0:T(8,128)(2,1)}) %reduce-scatter.2.cloned.1.call-update) | async-done | bytes 524304 | tf_op jit(solution)/shard_map/reduce_scatter | solution.py:181
  (107 shorter events, 5.5 us)
Async XLA Ops:
  6.5 7.4 %copy-start.7 = (f32[256,4]{0,1:T(4,128)S(1)}, f32[256,4]{0,1:T(4,128)}, u32[]{:S(2)}) copy-start(f32[256,4]{0,1:T(4,128)} %param.30) | copy-start | bytes 12292
  6.5 25.7 %all-gather.15.cloned.1.call-start = ((), (), s32[]{:S(2)}) async-start(), calls=%async_computation.1 | async-start | bytes 1572864 | tf_op jit(solution)/shard_map/all_gather | solution.py:130
  9.8 64.8 %all-gather.19.cloned.1.call-start = ((), (), s32[]{:S(2)}) async-start(), calls=%async_computation.3 | async-start | bytes 2228224 | tf_op jit(solution)/shard_map/all_gather | solution.py:114
  10.6 106.4 %all-gather.21.cloned.1.call-start = ((), (), s32[]{:S(2)}) async-start(), calls=%async_computation.4 | async-start | bytes 2228224 | tf_op jit(solution)/shard_map/all_gather | solution.py:112
  11.3 147.9 %all-gather.17.cloned.1.call-start = ((), (), s32[]{:S(2)}) async-start(), calls=%async_computation.2 | async-start | bytes 2228224 | tf_op jit(solution)/shard_map/all_gather | solution.py:113
  11.9 189.5 %all-gather.31.cloned.1.call-start = ((), (), s32[]{:S(2)}) async-start(), calls=%async_computation.9 | async-start | bytes 2228224 | tf_op jit(solution)/shard_map/all_gather | solution.py:118
  12.5 231.2 %all-gather.29.cloned.1.call-start = ((), (), s32[]{:S(2)}) async-start(), calls=%async_computation.8 | async-start | bytes 2228224 | tf_op jit(solution)/shard_map/all_gather | solution.py:117
  13.1 273.0 %all-gather.23.cloned.1.call-start = ((), (), s32[]{:S(2)}) async-start(), calls=%async_computation.5 | async-start | bytes 2228224 | tf_op jit(solution)/shard_map/all_gather | solution.py:115
  13.8 323.4 %all-gather.35.cloned.1.call-start = ((), (), s32[]{:S(2)}) async-start(), calls=%async_computation.12 | async-start | bytes 4456448 | tf_op jit(solution)/shard_map/all_gather | solution.py:15
  32.2 84.8 %copy-start.1 = (bf16[256,2048]{1,0:T(8,128)(2,1)S(1)}, bf16[256,2048]{1,0:T(8,128)(2,1)}, u32[]{:S(2)}) copy-start(bf16[256,2048]{1,0:T(8,128)(2,1)} %all-gather.15.cloned.1.call-done) | copy-start | bytes 3145732
  162.4 1.4 copy-start.8
  164.0 25.5 %copy-start.6 = (f32[3,512]{1,0:T(4,128)S(1)}, f32[3,512]{1,0:T(4,128)}, u32[]{:S(2)}) copy-start(f32[3,512]{1,0:T(4,128)} %param.33) | copy-start | bytes 18436
  186.6 0.7 copy-start
  187.4 56.3 %copy-start.2 = (bf16[256,2048]{1,0:T(8,128)(2,1)S(1)}, bf16[256,2048]{1,0:T(8,128)(2,1)}, u32[]{:S(2)}) copy-start(bf16[256,2048]{1,0:T(8,128)(2,1)} %all-gather.15.cloned.1.call-done) | copy-start | bytes 3145732
  187.4 191.5 %all-gather.25.cloned.1.call-start = ((), (), s32[]{:S(2)}) async-start(), calls=%async_computation.6 | async-start | bytes 2228224 | tf_op jit(solution)/shard_map/all_gather | solution.py:177
  188.1 233.7 %all-gather.27.cloned.1.call-start = ((), (), s32[]{:S(2)}) async-start(), calls=%async_computation.7 | async-start | bytes 2228224 | tf_op jit(solution)/shard_map/all_gather | solution.py:116
  188.7 274.7 %all-gather.33.cloned.1.call-start = ((), (), s32[]{:S(2)}) async-start(), calls=%async_computation.10 | async-start | bytes 2228224 | tf_op jit(solution)/shard_map/all_gather | solution.py:178
  189.4 300.1 %reduce-scatter.2.cloned.1.call-start = ((), (), s32[]{:S(2)}) async-start(), calls=%async_computation.11 | async-start | bytes 1572864 | tf_op jit(solution)/shard_map/reduce_scatter | solution.py:181
  246.0 43.2 %copy-start.4 = (bf16[256,512]{1,0:T(8,128)(2,1)}, bf16[256,512]{1,0:T(8,128)(2,1)S(1)}, u32[]{:S(2)}) copy-start(bf16[256,512]{1,0:T(8,128)(2,1)S(1)} %convolution_convert_fusion.1) | copy-start | bytes 786436
  246.0 59.3 %copy-start.3 = (f32[4,4,64,128]{3,2,0,1:T(8,128)S(1)}, f32[4,4,64,128]{3,2,0,1:T(8,128)}, u32[]{:S(2)}) copy-start(f32[4,4,64,128]{3,2,0,1:T(8,128)} %get-tuple-element.170) | copy-start | bytes 1572868
  246.0 60.7 %collective-permute-start = (bf16[2,2,512]{2,1,0:T(2,128)(2,1)S(1)}, bf16[2,2,512]{2,1,0:T(2,128)(2,1)S(1)}, u32[]{:S(2)}, u32[]{:S(2)}) collective-permute-start(bf16[2,2,512]{2,1,0:T(2,128)(2,1)S(1)} %pad_maximum_fusion), channel_id=1, source_target_pairs={{0,2},{2,4},{4,6},{6,8},{8,10},{10,12},{12,14},{14,16},{16,18},{18... | collective-permute-start | bytes 12296 | tf_op jit(solution)/shard_map/ppermute | solution.py:30
  307.8 47.4 %copy-start.5 = (f32[4,128,128]{2,1,0:T(8,128)S(1)}, f32[4,128,128]{2,1,0:T(8,128)}, u32[]{:S(2)}) copy-start(f32[4,128,128]{2,1,0:T(8,128)} %param.31) | copy-start | bytes 786436
  355.2 0.8 copy-start.9
Sparse Core Ops, SparseCore 0:
  10.0 22.2 all-gather.14
  34.4 40.1 all-gather.18
  76.8 40.1 all-gather.20
  119.0 40.1 all-gather.16
  161.2 40.1 all-gather.30
  203.5 40.1 all-gather.28
  245.8 40.1 all-gather.22
  288.2 48.9 all-gather.34
  339.4 39.4 all-gather.24
  380.9 40.8 all-gather.26
  423.9 39.4 all-gather.32
  468.5 21.0 reduce-scatter.1
where the time goes:
time: 499 us; the launch traced here: 496 us
  waiting for transfers between devices  390 us (78%)
  other arithmetic  36.6 us (7%)
  matrix products  32 us (6%)
  blocking collectives  16.1 us (3%)
  between operations  13.9 us (3%)
    all_gather x1, waiting for transfers between devices, on_device(): lax.all_gather(w_input, 'sp', axis=0, tiled=True)  42.4 us
    all_gather x1, waiting for transfers between devices, on_device(): lax.all_gather(out_conv, 'sp', axis=1, tiled=True)  41.7 us
    all_gather x1, waiting for transfers between devices, on_device(): lax.all_gather(w_bgate, 'sp', axis=0, tiled=True)  40.5 us
    all_gather x1, waiting for transfers between devices, on_device(): lax.all_gather(w_forget, 'sp', axis=0, tiled=True)  39.7 us
    all_gather x1, waiting for transfers between devices, on_device(): lax.all_gather(w_cgate, 'sp', axis=0, tiled=True)  39.6 us
    all_gather x1, waiting for transfers between devices, on_device(): lax.all_gather(w_query, 'sp', axis=0, tiled=True)  39.6 us
    all_gather x1, waiting for transfers between devices, on_device(): lax.all_gather(w_outgate, 'sp', axis=0, tiled=True)  37.7 us
    all_gather x1, waiting for transfers between devices, prefix(): pieces = jax.tree.map(lambda part: lax.all_gather(part, axis), value)  29.4 us
  transfers between devices with their start and end apart: 13, of which 12 were waited for; matrix products, arithmetic and copies ran while one was open for 13% of the time, Pallas kernels for 0%

commit v1 on v0

--- a/solution.py
+++ b/solution.py
@@ -1,6 +1,10 @@
+import functools
+
 import jax
 import jax.numpy as jnp
 from jax import lax
+from jax.experimental import pallas as pl
+from jax.experimental.pallas import tpu as pltpu
 from jax.sharding import PartitionSpec as P
 
 BLOCK = 64
@@ -188,6 +192,459 @@
     )
 
 
+MESH = pl.DeviceIdType.MESH
+f32, bf16 = jnp.float32, jnp.bfloat16
+
+
+def high_dot(a, b, dims):
+    return lax.dot_general(
+        a, b, (dims, ((), ())), precision=highest_precision, preferred_element_type=f32
+    )
+
+
+def sigmoid(v):
+    return 1.0 / (1.0 + jnp.exp(-v))
+
+
+def fused_kernel(
+    heads,
+    lines,
+    groups,
+    block,
+    tok_ref,
+    gain_ref,
+    w_ref,
+    o_ref,
+    gap_ref,
+    ed_ref,
+    start_ref,
+    sgain_ref,
+    taps_ref,
+    out_ref,
+    tg,
+    gw,
+    go,
+    ge,
+    proj,
+    gated,
+    mixed,
+    lifted,
+    lhs,
+    packet,
+    packets,
+    state,
+    part,
+    r0,
+    r1a,
+    r1b,
+    r2,
+    s_w,
+    s_o,
+    s_e,
+    s_t,
+    s_p,
+    sr_w,
+    sl_w,
+    sr_o,
+    sl_o,
+    v_w,
+    v_o,
+    v_e,
+    v_t,
+    v_p,
+    s_x0,
+    v_x0,
+    s_x1,
+    v_x1,
+    s_x2,
+    v_x2,
+):
+    s_me, t_me = lax.axis_index("sp"), lax.axis_index("tp")
+    q, r = s_me // heads, lax.rem(s_me, heads)
+    e_me = r * groups + t_me
+    every = heads * groups
+    rows = tok_ref.shape[0]
+    key = w_ref.shape[2] // 7
+    length = every * rows
+
+    def copy(src, dst, send, recv, dev):
+        return pltpu.make_async_remote_copy(
+            src_ref=src, dst_ref=dst, send_sem=send, recv_sem=recv, device_id=dev,
+            device_id_type=MESH,
+        )
+
+    def in_group(e):
+        return (q * heads + e // groups, lax.rem(e, groups))
+
+    def along(p):
+        return (p * heads + r, t_me)
+
+    barrier = pltpu.get_barrier_semaphore()
+    for d in range(1, every):
+        pl.semaphore_signal(
+            barrier, inc=1, device_id=in_group(lax.rem(e_me + d, every)), device_id_type=MESH
+        )
+    for d in range(1, lines):
+        pl.semaphore_signal(
+            barrier, inc=1, device_id=along(lax.rem(q + d, lines)), device_id_type=MESH
+        )
+    pl.semaphore_wait(barrier, every - 1 + lines - 1)
+
+    has_right, has_left = q + 1 < lines, q > 0
+    right = along(lax.rem(q + 1, lines))
+    left = along(lax.rem(q + lines - 1, lines))
+
+    def moves(src, dst, send_r, send_l, recv, s):
+        return (
+            copy(src, dst.at[s], send_r.at[s], recv.at[s], right),
+            copy(src, dst.at[s], send_l.at[s], recv.at[s], left),
+        )
+
+    def forward(src, dst, send_r, send_l, recv, s, to_right=True, to_left=True):
+        go_right, go_left = moves(src, dst, send_r, send_l, recv, s)
+        if to_right:
+            pl.when(has_right)(go_right.start)
+        if to_left:
+            pl.when(has_left)(go_left.start)
+
+    W = (gw, sr_w, sl_w, v_w)
+    O = (go, sr_o, sl_o, v_o)
+
+    def swaps(ref, dst, send, recv):
+        found = []
+        for j in range(1, heads):
+            other = lax.rem(r + j, heads)
+            found.append(
+                copy(ref.at[other], dst, send.at[j], recv, (q * heads + other, t_me))
+            )
+        return found
+
+    w_swaps = swaps(w_ref, gw.at[s_me], s_w, v_w.at[s_me])
+    e_swaps = swaps(ed_ref, ge.at[r], s_e, v_e.at[r])
+    o_swaps = swaps(o_ref, go.at[s_me], s_o, v_o.at[s_me])
+    t_sends = []
+    for d in range(1, every):
+        t_sends.append(
+            copy(tok_ref, tg.at[e_me], s_t.at[d], v_t.at[e_me], in_group(lax.rem(e_me + d, every)))
+        )
+    for c in w_swaps:
+        c.start()
+    forward(w_ref.at[r], *W, s_me)
+    for c in e_swaps + o_swaps + t_sends:
+        c.start()
+    gw[s_me] = w_ref[r]
+    go[s_me] = o_ref[r]
+    ge[r] = ed_ref[r]
+    tg[e_me] = tok_ref[...]
+
+    def arrived(dst, recv, s):
+        copy(dst.at[s], dst.at[s], s_p.at[0], recv.at[s], right).wait_recv()
+
+    def relay_own(kind):
+        for j in range(1, heads):
+            s = q * heads + lax.rem(r + j, heads)
+            arrived(kind[0], kind[3], s)
+            forward(kind[0].at[s], *kind, s)
+
+    def relay(kind, k):
+        for j in range(heads):
+            rr = lax.rem(r + j, heads)
+
+            @pl.when(q >= k)
+            def _():
+                s = (q - k) * heads + rr
+                arrived(kind[0], kind[3], s)
+                forward(kind[0].at[s], *kind, s, to_left=False)
+
+            @pl.when(q + k < lines)
+            def _():
+                s = (q + k) * heads + rr
+                arrived(kind[0], kind[3], s)
+                forward(kind[0].at[s], *kind, s, to_right=False)
+
+    relay_own(W)
+    for k in range(1, lines):
+        relay(W, k)
+        if k == lines - 2:
+            forward(o_ref.at[r], *O, s_me)
+            relay_own(O)
+
+    for d in range(1, every):
+        arrived(tg, v_t, lax.rem(e_me + d, every))
+
+    step = 16
+
+    def norm(i, _):
+        e = i // (rows // step)
+        at = pl.ds(pl.multiple_of(lax.rem(i, rows // step) * step, step), step)
+        x = tg[e, at, :].astype(f32)
+        tg[e, at, :] = (x * rms_scale(x) * gain_ref[...]).astype(bf16)
+        return 0
+
+    lax.fori_loop(0, length // step, norm, 0)
+
+    depth = heads * w_ref.shape[1]
+    tall = 2 * rows
+
+    def project(i, _):
+        at = pl.ds(pl.multiple_of(i * tall, tall), tall)
+        acc = jnp.zeros((tall, 7 * key), f32)
+        for p in range(lines):
+            x = tg[pl.ds(i * 2, 2), :, pl.ds(p * depth, depth)].reshape(tall, depth)
+            w = gw[pl.ds(p * heads, heads)].reshape(depth, 7 * key)
+            acc = acc + jnp.dot(x, w, preferred_element_type=f32)
+        proj[at, :] = acc.astype(bf16)
+        return 0
+
+    lax.fori_loop(0, length // tall, project, 0)
+    for k in range(1, lines - 1):
+        relay(O, k)
+    for j in range(1, heads):
+        arrived(ge, v_e, lax.rem(r + j, heads))
+
+    def column(at, number):
+        return proj[at, number * key : (number + 1) * key].astype(f32)
+
+    pad = 8
+    blocks = length // block
+    per = blocks // heads
+    tri = (
+        lax.broadcasted_iota(jnp.int32, (block, block), 0)
+        >= lax.broadcasted_iota(jnp.int32, (block, block), 1)
+    ).astype(f32)
+    wide = (
+        lax.broadcasted_iota(jnp.int32, (block, key), 0)
+        >= lax.broadcasted_iota(jnp.int32, (block, key), 1)
+    ).astype(f32)
+    gap = gap_ref[pl.ds(r, 1), :]
+    packet[...] = jnp.zeros_like(packet)
+
+    def advance(b, _):
+        at = pl.ds(pl.multiple_of(b * block, block), block)
+        query = column(at, 0)
+        query = query * sigmoid(query)
+        write = gap * sigmoid(-column(at, 1))
+        values = column(at, 2)
+        extra = ge[b // per, pl.ds(lax.rem(b, per), 1), :]
+        run = high_dot(tri, jnp.log1p(-write), ((1,), (0,))) + jnp.sum(
+            wide * extra, axis=1, keepdims=True
+        )
+        final = run[block - 1 : block, :]
+        middle = 0.5 * final
+        scores = tri * high_dot(
+            query * jnp.exp(run - middle), write * jnp.exp(middle - run), ((1,), (1,))
+        )
+        before = packet[:key, :]
+        offset = packet[key : key + 1, :]
+        lift = query * jnp.exp(run)
+        mixed[at, :] = high_dot(scores, values, ((1,), (0,))) + high_dot(
+            lift, before, ((1,), (1,))
+        )
+        lifted[at, :] = lift * jnp.exp(offset)
+        packet[:key, :] = before * jnp.exp(final) + high_dot(
+            values, write * jnp.exp(final - run), ((0,), (0,))
+        )
+        packet[key : key + pad, :] = jnp.broadcast_to(offset + final, (pad, key))
+        gated[pl.ds(pl.multiple_of(b * block + pad, pad), block), :] = column(at, 5) * column(at, 6)
+        return 0
+
+    lax.fori_loop(0, blocks, advance, 0)
+    packet[key + pad : key + 2 * pad, :] = gated[length : length + pad, :]
+
+    def packet_to(d):
+        return copy(
+            packet, packets.at[q], s_p.at[d], v_p.at[q], along(lax.rem(q + d, lines))
+        )
+
+    for d in range(1, lines):
+        pl.when(q + d < lines)(packet_to(d).start)
+    state[...] = start_ref[r].T
+    gated[:pad, :] = jnp.zeros((pad, key), f32)
+    relay(O, lines - 1)
+    for p in range(lines - 1):
+
+        @pl.when(p < q)
+        def _():
+            arrived(packets, v_p, p)
+            state[...] = state[...] * jnp.exp(packets[p, key : key + 1, :]) + packets[p, :key, :]
+
+        @pl.when(p + 1 == q)
+        def _():
+            gated[:pad, :] = packets[p, key + pad : key + 2 * pad, :]
+
+    taps = taps_ref[r]
+    for i in range(every):
+        lo = i * rows
+        at = pl.ds(lo, rows)
+        m = mixed[at, :] + high_dot(lifted[at, :], state[...], ((1,), (1,)))
+        gate = column(at, 3)
+        rec = m * rms_scale(m) * sgain_ref[...] * (gate * sigmoid(gate))
+        conv = (
+            taps[0:1] * gated[lo + pad - 2 : lo + pad - 2 + rows, :]
+            + taps[1:2] * gated[lo + pad - 1 : lo + pad - 1 + rows, :]
+            + taps[2:3] * gated[lo + pad : lo + pad + rows, :]
+        )
+        lhs[at, :key] = rec.astype(bf16)
+        lhs[at, key:] = (column(at, 4) * conv).astype(bf16)
+
+    span = o_ref.shape[2]
+    width = span * heads * lines
+    half = width // 2
+
+    def expand(i, _):
+        for p in range(heads * lines // 2):
+            w = jnp.concatenate([go[2 * p], go[2 * p + 1]], axis=1)
+            part[i, :, 2 * span * p : 2 * span * (p + 1)] = jnp.dot(
+                lhs[pl.ds(pl.multiple_of(i * rows, rows), rows), :], w, preferred_element_type=f32
+            ).astype(bf16)
+        return 0
+
+    lax.fori_loop(0, every, expand, 0)
+
+    y, c = r // 2, lax.rem(r, 2)
+    cc, yy, xx = 1 - c, 1 - y, 1 - t_me
+
+    def slot(y, c, x):
+        return (y * 2 + c) * groups + x
+
+    core = (q * heads + y * 2 + cc, t_me)
+    over_y = (q * heads + yy * 2 + c, t_me)
+    over_x = (s_me, xx)
+    lo, hi = pl.ds(0, half), pl.ds(half, half)
+    first = []
+    for a in range(2):
+        for b in range(2):
+            n = 2 * a + b
+            first.append(copy(part.at[slot(a, cc, b)], r0.at[n], s_x0.at[n], v_x0.at[n], core))
+    for d in first:
+        d.start()
+
+    def add(e, cols, other):
+        return part[e, :, cols].astype(f32) + other.astype(f32)
+
+    for d in first:
+        d.wait()
+    for a in range(2):
+        for b in range(2):
+            e = slot(a, c, b)
+            part[e] = (part[e].astype(f32) + r0[2 * a + b].astype(f32)).astype(bf16)
+    second = []
+    for b in range(2):
+        second.append(
+            copy(part.at[slot(yy, c, b), :, lo], r1a.at[b], s_x1.at[b], v_x1.at[b], over_y)
+        )
+        second.append(
+            copy(part.at[slot(b, c, xx), :, hi], r1b.at[b], s_x1.at[2 + b], v_x1.at[2 + b], over_x)
+        )
+    for d in second:
+        d.start()
+    for d in second:
+        d.wait()
+    part[slot(y, c, xx), :, lo] = add(slot(y, c, xx), lo, r1a[xx]).astype(bf16)
+    part[slot(yy, c, t_me), :, hi] = add(slot(yy, c, t_me), hi, r1b[yy]).astype(bf16)
+    third = [
+        copy(part.at[slot(y, c, xx), :, lo], r2.at[0], s_x2.at[0], v_x2.at[0], over_x),
+        copy(part.at[slot(yy, c, t_me), :, hi], r2.at[1], s_x2.at[1], v_x2.at[1], over_y),
+    ]
+    for d in third:
+        d.start()
+    mine = slot(y, c, t_me)
+    for d in third:
+        d.wait()
+    out_ref[:, lo] = (add(mine, lo, r1a[t_me]) + r2[0].astype(f32)).astype(bf16)
+    out_ref[:, hi] = (add(mine, hi, r1b[y]) + r2[1].astype(f32)).astype(bf16)
+
+    for c in w_swaps + e_swaps + o_swaps + t_sends:
+        c.wait_send()
+    for d in range(1, lines):
+        pl.when(q + d < lines)(packet_to(d).wait_send)
+
+    for kind in (W, O):
+        for p in range(lines):
+            for j in range(heads):
+                s = p * heads + j
+                go_right, go_left = moves(kind[0].at[s], *kind, s)
+                pl.when(jnp.logical_and(has_right, p <= q))(go_right.wait_send)
+                pl.when(jnp.logical_and(has_left, p >= q))(go_left.wait_send)
+
+
+def fused(heads, lines, groups, *args):
+    (tokens, norm_gain, w_query, w_forget, w_input, w_outgate, w_bgate, w_cgate, w_value,
+     floor_gap, extra_decay, start_state, state_gain, conv_taps, out_rec, out_conv) = args
+    rows, model = tokens.shape
+    depth = w_query.shape[0]
+    key = floor_gap.shape[1]
+    span = out_rec.shape[1]
+    every = heads * groups
+    length = every * rows
+    sp = heads * lines
+    pad = 8
+
+    def by_head(tensor):
+        return tensor.reshape(tensor.shape[0], heads, key).transpose(1, 0, 2)
+
+    weights = jnp.concatenate(
+        [by_head(w) for w in (w_query, w_forget, w_input, w_outgate, w_bgate, w_cgate, w_value)],
+        axis=2,
+    )
+    outs = jnp.concatenate(
+        [out_rec.reshape(heads, key, span), out_conv.reshape(heads, key, span)], axis=1
+    )
+    per = extra_decay.shape[0] // BLOCK
+    extra = extra_decay.T.reshape(heads, per, BLOCK)
+    extra = jnp.pad(extra, ((0, 0), (0, pad - per), (0, key - BLOCK)))
+    taps = jnp.pad(by_head(conv_taps), ((0, 0), (0, pad - conv_taps.shape[0]), (0, 0)))
+    dma = pltpu.SemaphoreType.DMA
+    half = model // 2
+    scratch = [
+        pltpu.VMEM((every, rows, model), bf16),
+        pltpu.VMEM((sp, depth, 7 * key), bf16),
+        pltpu.VMEM((sp, 2 * key, span), bf16),
+        pltpu.VMEM((heads, pad, key), f32),
+        pltpu.VMEM((length, 7 * key), bf16),
+        pltpu.VMEM((length + pad, key), f32),
+        pltpu.VMEM((length, key), f32),
+        pltpu.VMEM((length, key), f32),
+        pltpu.VMEM((length, 2 * key), bf16),
+        pltpu.VMEM((key + 2 * pad, key), f32),
+        pltpu.VMEM((lines, key + 2 * pad, key), f32),
+        pltpu.VMEM((key, key), f32),
+        pltpu.VMEM((every, rows, model), bf16),
+        pltpu.VMEM((every // 2, rows, model), bf16),
+        pltpu.VMEM((2, rows, half), bf16),
+        pltpu.VMEM((2, rows, half), bf16),
+        pltpu.VMEM((2, rows, half), bf16),
+        dma((heads,)), dma((heads,)), dma((heads,)), dma((every,)), dma((lines,)),
+        dma((sp,)), dma((sp,)), dma((sp,)), dma((sp,)),
+        dma((sp,)), dma((sp,)), dma((heads,)), dma((every,)), dma((lines,)),
+        dma((4,)), dma((4,)), dma((4,)), dma((4,)), dma((2,)), dma((2,)),
+    ]
+    return pl.pallas_call(
+        functools.partial(fused_kernel, heads, lines, groups, BLOCK),
+        out_shape=jax.ShapeDtypeStruct((rows, model), bf16),
+        in_specs=[pl.BlockSpec(memory_space=pltpu.VMEM)] * 9,
+        out_specs=pl.BlockSpec(memory_space=pltpu.VMEM),
+        scratch_shapes=scratch,
+        compiler_params=pltpu.CompilerParams(
+            collective_id=0, has_side_effects=True, vmem_limit_bytes=60 * 1024 * 1024
+        ),
+        name="mixer",
+    )(tokens, norm_gain[None], weights, outs, floor_gap, extra, start_state, state_gain[None], taps)
+
+
+def per_device(sp, tp, *args):
+    heads = args[9].shape[0]
+    fits = (
+        heads == 4 and tp == 2 and sp % heads == 0
+        and args[14].shape[1] % 128 == 0
+        and args[13].shape[1] == heads * args[9].shape[1]
+        and args[10].shape[0] % BLOCK == 0
+    )
+    if not fits:
+        return on_device(*args)
+    return fused(heads, sp // heads, tp, *args)
+
+
 def solution(mesh):
     placed = (
         P(("sp", "tp"), None),
@@ -208,5 +665,5 @@
         P("tp", "sp"),
     )
     return jax.shard_map(
-        on_device, mesh=mesh, in_specs=placed, out_specs=P(("sp", "tp"), None), check_vma=False
-    )
+        functools.partial(per_device, mesh.shape["sp"], mesh.shape["tp"]), mesh=mesh, in_specs=placed, out_specs=P(("sp", "tp"), None), check_vma=False
+    )

time: 499 us -> 151 us (0.30)
  waiting for transfers between devices: 390 us -> 0 us
  Pallas kernels: 0 us -> 138 us
  other arithmetic: 36.6 us -> 0.72 us
  matrix products: 32 us -> 0 us
  blocking collectives: 16.1 us -> 0 us
  between operations: 13.9 us -> 0.22 us
  local copies, waits for them, and re-layouts: 4.17 us -> 11.5 us
    all_gather x11 -> x0, waiting for transfers between devices: 363 us -> none  [the longest x1 42.4 us: on_device(): lax.all_gather(w_input, 'sp', axis=0, tiled=True)]
    pallas_call x0 -> x1, Pallas kernels: none -> 138 us  [fused(): pl.pallas_call(functools.partial(fused_kernel, heads, lines, groups, BLOC...]
    dot_general x21 -> x0, matrix products: 32 us -> none  [the longest x6 16.2 us: project(): jnp.dot(shard_rows, matrix, preferred_element_type=jnp.float32)]
    reduce_scatter x1 -> x0, waiting for transfers between devices: 21.2 us -> none  [on_device(): lax.psum_scatter((product + jnp.dot(short_out, conv_weight, preferred_ele...]
    select_n x30 -> x0, other arithmetic: 17.5 us -> none  [hop(): jnp.where(position < mine, new, old)]
    all_gather x1 -> x0, blocking collectives: 16.1 us -> none  [prefix(): pieces = jax.tree.map(lambda part: lax.all_gather(part, axis), value)]
    reduce_sum x5 -> x0, other arithmetic: 14.8 us -> none  [the longest x4 13.6 us: advance(): jnp.sum(query_block[:, :, None, :] * write_blk[:, None, :, :] * decays, a...]
    unnamed x21 -> x36, local copies, waits for them, and re-layouts: 0.74 us -> 9.28 us
  transfers between devices with their start and end apart: 13 -> 0, of which waited for: 12 -> 0; matrix products, arithmetic and copies ran while one was open for 13% -> 0% of each run, Pallas kernels for 0% -> 0%
where the time goes in v1:
time: 151 us
  Pallas kernels  138 us (91%)
  local copies, waits for them, and re-layouts  11.5 us (8%)
    pallas_call x1, Pallas kernels, fused(): pl.pallas_call(functools.partial(fused_kernel, heads, lines, groups, BLOC...  138 us
    unnamed x36, local copies, waits for them, and re-layouts  9.28 us

profile of v1, /device:TPU:24, one launch (start us, length us, event | category | flops | bytes accessed | tf_op | source)
XLA Modules:
  0.0 150.9 jit_solution(14586304771923795540)
XLA Ops:
  0.0 1.0 copy.17
  1.0 0.0 copy-start.1
  1.0 0.1 copy.18
  1.2 0.7 copy-done.1
  1.9 0.1 copy.19
  2.1 0.0 copy-start.2
  2.1 0.1 copy.20
  2.2 0.7 copy-done.2
  3.0 0.1 copy.21
  3.1 0.0 copy-start.3
  3.1 0.1 copy.22
  3.3 0.7 copy-done.3
  4.0 0.1 copy.23
  4.1 0.0 copy-start.4
  4.1 0.1 copy.24
  4.3 0.7 copy-done.4
  5.0 0.1 copy.25
  5.2 0.0 copy-start.5
  5.2 0.1 copy.26
  5.3 0.7 copy-done.5
  6.1 0.1 copy.27
  6.2 0.0 copy-start.6
  6.2 0.1 copy.28
  6.4 0.7 copy-done.6
  7.1 0.1 copy.29
  7.2 0.1 copy.30
  7.4 0.0 copy-start.7
  7.4 0.0 copy-start.8
  7.4 0.0 copy-start
  7.4 0.8 copy-done.7
  8.3 0.2 copy-done.8
  8.5 0.0 copy-start.10
  8.5 0.7 pad_maximum_fusion.o_ref
  9.2 0.0 copy-done.10
  9.2 0.1 reshape.42
  9.3 0.0 copy-start.9
  9.3 0.6 pad.8.ed_ref
  9.9 0.1 copy-done.9
  10.0 0.6 pad.9.taps_ref
  10.6 0.0 copy-done
  10.6 138.5 %mixer.1 = bf16[128,2048]{1,0:T(8,128)(2,1)} custom-call(bf16[128,2048]{1,0:T(8,128)(2,1)} %tok_ref.1, f32[1,2048]{1,0:T(1,128)} %bitcast.38, bf16[4,128,896]{2,1,0:T(8,128)(2,1)} %copy-done, bf16[4,256,128]{2,1,0:T(8,128)(2,1)} %pad_maximum_fusion.o_ref, f32[4,128]{1,0:T(4,128)} %gap_ref.1, f32[4,8,128]{2,1,0:T(8,128)} %pad.8.ed_ref, ...), custom_call_target="tpu_custom_call" | custom-call | tf_op jit(solution)/shard_map/mixer/pallas_call | solution.py:622
  149.0 1.9 %copy.38 = bf16[128,2048]{1,0:T(8,128)(2,1)} copy(bf16[128,2048]{1,0:T(8,128)(2,1)} %mixer.1) | data formatting | bytes 1048576
  (7 shorter events, 0.2 us)
Async XLA Ops:
  1.0 0.9 copy-start.1
  2.1 0.9 copy-start.2
  3.1 0.9 copy-start.3
  4.1 0.9 copy-start.4
  5.2 0.9 copy-start.5
  6.2 0.9 copy-start.6
  7.4 0.9 copy-start.7
  7.4 1.1 copy-start.8
  7.4 3.1 %copy-start = (bf16[4,128,896]{2,1,0:T(8,128)(2,1)}, bf16[4,128,896]{2,1,0:T(8,128)(2,1)S(1)}, u32[]{:S(2)}) copy-start(bf16[4,128,896]{2,1,0:T(8,128)(2,1)S(1)} %bitcast_dynamic-update-slice_fusion.w_ref) | copy-start | bytes 2752516
  8.5 0.7 copy-start.10
  9.3 0.7 copy-start.9

commit v2 on v1

--- a/solution.py
+++ b/solution.py
@@ -211,16 +211,21 @@
     lines,
     groups,
     block,
-    tok_ref,
+    tok_in,
     gain_ref,
-    w_ref,
-    o_ref,
+    w_ins,
+    rec_in,
+    conv_in,
     gap_ref,
     ed_ref,
     start_ref,
     sgain_ref,
     taps_ref,
     out_ref,
+    tok_ref,
+    w_ref,
+    o_ref,
+    normed,
     tg,
     gw,
     go,
@@ -229,7 +234,6 @@
     gated,
     mixed,
     lifted,
-    lhs,
     packet,
     packets,
     state,
@@ -258,6 +262,8 @@
     v_x1,
     s_x2,
     v_x2,
+    d_w,
+    d_o,
 ):
     s_me, t_me = lax.axis_index("sp"), lax.axis_index("tp")
     q, r = s_me // heads, lax.rem(s_me, heads)
@@ -279,6 +285,24 @@
     def along(p):
         return (p * heads + r, t_me)
 
+    staged = []
+    for j in range(heads):
+        h = lax.rem(r + j, heads)
+        for number, w_in in enumerate(w_ins):
+            staged.append(
+                pltpu.make_async_copy(
+                    w_in.at[:, pl.ds(pl.multiple_of(h * key, key), key)],
+                    w_ref.at[h, :, number * key : (number + 1) * key],
+                    d_w.at[h],
+                )
+            )
+    staged.append(pltpu.make_async_copy(tok_in, tok_ref, d_o.at[0]))
+    for h in range(heads):
+        at = pl.ds(h * key, key)
+        staged.append(pltpu.make_async_copy(rec_in.at[at], o_ref.at[h, :key], d_o.at[1]))
+        staged.append(pltpu.make_async_copy(conv_in.at[at], o_ref.at[h, key:], d_o.at[1]))
+    for c in staged:
+        c.start()
     barrier = pltpu.get_barrier_semaphore()
     for d in range(1, every):
         pl.semaphore_signal(
@@ -322,20 +346,39 @@
     w_swaps = swaps(w_ref, gw.at[s_me], s_w, v_w.at[s_me])
     e_swaps = swaps(ed_ref, ge.at[r], s_e, v_e.at[r])
     o_swaps = swaps(o_ref, go.at[s_me], s_o, v_o.at[s_me])
-    t_sends = []
-    for d in range(1, every):
-        t_sends.append(
-            copy(tok_ref, tg.at[e_me], s_t.at[d], v_t.at[e_me], in_group(lax.rem(e_me + d, every)))
-        )
-    for c in w_swaps:
-        c.start()
+    y, c = r // 2, lax.rem(r, 2)
+    cc, yy, xx = 1 - c, 1 - y, 1 - t_me
+
+    def slot(y, c, x):
+        return (y * 2 + c) * groups + x
+
+    core = (q * heads + y * 2 + cc, t_me)
+    over_y = (q * heads + yy * 2 + c, t_me)
+    over_x = (s_me, xx)
+    over_xy = (q * heads + yy * 2 + c, xx)
+    t_sends = [
+        copy(tok_ref, tg.at[e_me], s_t.at[n], v_t.at[e_me], dev)
+        for n, dev in enumerate((core, over_x, over_y, over_xy))
+    ]
+    t_passes = [
+        copy(tg.at[e], tg.at[e], s_t.at[4 + n], v_t.at[e], core)
+        for n, e in enumerate((slot(y, c, xx), slot(yy, c, t_me), slot(yy, c, xx)))
+    ]
+    pltpu.make_async_copy(w_ref.at[r], w_ref.at[r], d_w.at[r]).wait()
     forward(w_ref.at[r], *W, s_me)
-    for c in e_swaps + o_swaps + t_sends:
-        c.start()
+    for j in range(1, heads):
+        h = lax.rem(r + j, heads)
+        pltpu.make_async_copy(w_ref.at[h], w_ref.at[h], d_w.at[h]).wait()
+        w_swaps[j - 1].start()
+    pltpu.make_async_copy(tok_in, tok_ref, d_o.at[0]).wait()
+    for d in e_swaps + t_sends:
+        d.start()
+    pltpu.make_async_copy(o_ref, o_ref, d_o.at[1]).wait()
+    for d in o_swaps:
+        d.start()
     gw[s_me] = w_ref[r]
     go[s_me] = o_ref[r]
     ge[r] = ed_ref[r]
-    tg[e_me] = tok_ref[...]
 
     def arrived(dst, recv, s):
         copy(dst.at[s], dst.at[s], s_p.at[0], recv.at[s], right).wait_recv()
@@ -346,7 +389,41 @@
             arrived(kind[0], kind[3], s)
             forward(kind[0].at[s], *kind, s)
 
-    def relay(kind, k):
+    step = 16
+
+    def norm(e, src):
+        def body(i, _):
+            at = pl.ds(pl.multiple_of(i * step, step), step)
+            x = src[at, :].astype(f32)
+            normed[e, at, :] = (x * rms_scale(x) * gain_ref[...]).astype(bf16)
+            return 0
+
+        lax.fori_loop(0, rows // step, body, 0)
+
+    def take(e):
+        arrived(tg, v_t, e)
+        norm(e, tg.at[e])
+
+    def hand_on(n, e):
+        arrived(tg, v_t, e)
+        t_passes[n].start()
+
+    by_x, by_y, by_xy = slot(y, c, xx), slot(yy, c, t_me), slot(yy, c, xx)
+    chores = [
+        lambda: norm(e_me, tok_ref),
+        lambda: take(slot(y, cc, t_me)),
+        lambda: hand_on(0, by_x),
+        lambda: norm(by_x, tg.at[by_x]),
+        lambda: hand_on(1, by_y),
+        lambda: norm(by_y, tg.at[by_y]),
+        lambda: take(slot(y, cc, xx)),
+        lambda: take(slot(yy, cc, t_me)),
+        lambda: hand_on(2, by_xy),
+        lambda: norm(by_xy, tg.at[by_xy]),
+        lambda: take(slot(yy, cc, xx)),
+    ]
+
+    def relay(kind, k, between):
         for j in range(heads):
             rr = lax.rem(r + j, heads)
 
@@ -362,26 +439,35 @@
                 arrived(kind[0], kind[3], s)
                 forward(kind[0].at[s], *kind, s, to_right=False)
 
+            if between:
+                between.pop(0)()
+
+    def relay_inner(kind, k, inner):
+        for j in range(heads):
+            rr = lax.rem(r + j, heads)
+
+            @pl.when(jnp.logical_and(q >= k, has_right == inner))
+            def _():
+                s = (q - k) * heads + rr
+                arrived(kind[0], kind[3], s)
+                forward(kind[0].at[s], *kind, s, to_left=False)
+
+            @pl.when(jnp.logical_and(q + k < lines, has_left == inner))
+            def _():
+                s = (q + k) * heads + rr
+                arrived(kind[0], kind[3], s)
+                forward(kind[0].at[s], *kind, s, to_right=False)
+
     relay_own(W)
     for k in range(1, lines):
-        relay(W, k)
+        relay(W, k, chores)
         if k == lines - 2:
             forward(o_ref.at[r], *O, s_me)
             relay_own(O)
-
-    for d in range(1, every):
-        arrived(tg, v_t, lax.rem(e_me + d, every))
-
-    step = 16
-
-    def norm(i, _):
-        e = i // (rows // step)
-        at = pl.ds(pl.multiple_of(lax.rem(i, rows // step) * step, step), step)
-        x = tg[e, at, :].astype(f32)
-        tg[e, at, :] = (x * rms_scale(x) * gain_ref[...]).astype(bf16)
-        return 0
-
-    lax.fori_loop(0, length // step, norm, 0)
+    for k in range(1, lines):
+        relay_inner(O, k, True)
+    while chores:
+        chores.pop(0)()
 
     depth = heads * w_ref.shape[1]
     tall = 2 * rows
@@ -390,15 +476,13 @@
         at = pl.ds(pl.multiple_of(i * tall, tall), tall)
         acc = jnp.zeros((tall, 7 * key), f32)
         for p in range(lines):
-            x = tg[pl.ds(i * 2, 2), :, pl.ds(p * depth, depth)].reshape(tall, depth)
+            x = normed[pl.ds(i * 2, 2), :, pl.ds(p * depth, depth)].reshape(tall, depth)
             w = gw[pl.ds(p * heads, heads)].reshape(depth, 7 * key)
             acc = acc + jnp.dot(x, w, preferred_element_type=f32)
         proj[at, :] = acc.astype(bf16)
         return 0
 
     lax.fori_loop(0, length // tall, project, 0)
-    for k in range(1, lines - 1):
-        relay(O, k)
     for j in range(1, heads):
         arrived(ge, v_e, lax.rem(r + j, heads))
 
@@ -460,7 +544,6 @@
         pl.when(q + d < lines)(packet_to(d).start)
     state[...] = start_ref[r].T
     gated[:pad, :] = jnp.zeros((pad, key), f32)
-    relay(O, lines - 1)
     for p in range(lines - 1):
 
         @pl.when(p < q)
@@ -472,90 +555,88 @@
         def _():
             gated[:pad, :] = packets[p, key + pad : key + 2 * pad, :]
 
-    taps = taps_ref[r]
-    for i in range(every):
-        lo = i * rows
-        at = pl.ds(lo, rows)
+    for k in range(1, lines):
+        relay_inner(O, k, False)
+    taps = taps_ref[:, pl.ds(pl.multiple_of(r * key, key), key)]
+    span = o_ref.shape[2]
+    width = span * heads * lines
+    half = width // 2
+
+    def finish(e):
+        start = pl.multiple_of(e * rows, rows)
+        at = pl.ds(start, rows)
         m = mixed[at, :] + high_dot(lifted[at, :], state[...], ((1,), (1,)))
         gate = column(at, 3)
         rec = m * rms_scale(m) * sgain_ref[...] * (gate * sigmoid(gate))
+        near = gated[pl.ds(start, rows + pad), :]
         conv = (
-            taps[0:1] * gated[lo + pad - 2 : lo + pad - 2 + rows, :]
-            + taps[1:2] * gated[lo + pad - 1 : lo + pad - 1 + rows, :]
-            + taps[2:3] * gated[lo + pad : lo + pad + rows, :]
-        )
-        lhs[at, :key] = rec.astype(bf16)
-        lhs[at, key:] = (column(at, 4) * conv).astype(bf16)
-
-    span = o_ref.shape[2]
-    width = span * heads * lines
-    half = width // 2
-
-    def expand(i, _):
+            taps[0:1] * near[pad - 2 : pad - 2 + rows]
+            + taps[1:2] * near[pad - 1 : pad - 1 + rows]
+            + taps[2:3] * near[pad : pad + rows]
+        )
+        left_side = jnp.concatenate(
+            [rec.astype(bf16), (column(at, 4) * conv).astype(bf16)], axis=1
+        )
         for p in range(heads * lines // 2):
             w = jnp.concatenate([go[2 * p], go[2 * p + 1]], axis=1)
-            part[i, :, 2 * span * p : 2 * span * (p + 1)] = jnp.dot(
-                lhs[pl.ds(pl.multiple_of(i * rows, rows), rows), :], w, preferred_element_type=f32
+            part[e, :, 2 * span * p : 2 * span * (p + 1)] = jnp.dot(
+                left_side, w, preferred_element_type=f32
             ).astype(bf16)
-        return 0
-
-    lax.fori_loop(0, every, expand, 0)
-
-    y, c = r // 2, lax.rem(r, 2)
-    cc, yy, xx = 1 - c, 1 - y, 1 - t_me
-
-    def slot(y, c, x):
-        return (y * 2 + c) * groups + x
-
-    core = (q * heads + y * 2 + cc, t_me)
-    over_y = (q * heads + yy * 2 + c, t_me)
-    over_x = (s_me, xx)
+
     lo, hi = pl.ds(0, half), pl.ds(half, half)
+    order = ((yy, xx), (yy, t_me), (y, xx), (y, t_me))
     first = []
-    for a in range(2):
-        for b in range(2):
-            n = 2 * a + b
-            first.append(copy(part.at[slot(a, cc, b)], r0.at[n], s_x0.at[n], v_x0.at[n], core))
-    for d in first:
-        d.start()
+    for a, b in order:
+        n = 2 * a + b
+        finish(slot(a, cc, b))
+        first.append(copy(part.at[slot(a, cc, b)], r0.at[n], s_x0.at[n], v_x0.at[n], core))
+        first[-1].start()
 
     def add(e, cols, other):
         return part[e, :, cols].astype(f32) + other.astype(f32)
 
-    for d in first:
-        d.wait()
-    for a in range(2):
-        for b in range(2):
-            e = slot(a, c, b)
-            part[e] = (part[e].astype(f32) + r0[2 * a + b].astype(f32)).astype(bf16)
-    second = []
-    for b in range(2):
-        second.append(
-            copy(part.at[slot(yy, c, b), :, lo], r1a.at[b], s_x1.at[b], v_x1.at[b], over_y)
-        )
-        second.append(
-            copy(part.at[slot(b, c, xx), :, hi], r1b.at[b], s_x1.at[2 + b], v_x1.at[2 + b], over_x)
-        )
-    for d in second:
-        d.start()
-    for d in second:
-        d.wait()
-    part[slot(y, c, xx), :, lo] = add(slot(y, c, xx), lo, r1a[xx]).astype(bf16)
-    part[slot(yy, c, t_me), :, hi] = add(slot(yy, c, t_me), hi, r1b[yy]).astype(bf16)
+    def arrived_hi(b):
+        copy(r1b.at[b], r1b.at[b], s_p.at[0], v_x1.at[2 + b], right).wait_recv()
+
+    def to_y(b):
+        return copy(part.at[slot(yy, c, b), :, lo], r1a.at[b], s_x1.at[b], v_x1.at[b], over_y)
+
+    def to_x(b):
+        return copy(
+            part.at[slot(b, c, xx), :, hi], r1b.at[b], s_x1.at[2 + b], v_x1.at[2 + b], over_x
+        )
+
+    second = [to_y(xx), to_x(yy), to_y(t_me), to_x(y)]
+    sends = [second[:2], second[2:3], second[3:], []]
+    for (a, b), ready, d in zip(order, sends, first):
+        e = slot(a, c, b)
+        finish(e)
+        d.wait_recv()
+        part[e] = (part[e].astype(f32) + r0[2 * a + b].astype(f32)).astype(bf16)
+        for s in ready:
+            s.start()
     third = [
         copy(part.at[slot(y, c, xx), :, lo], r2.at[0], s_x2.at[0], v_x2.at[0], over_x),
         copy(part.at[slot(yy, c, t_me), :, hi], r2.at[1], s_x2.at[1], v_x2.at[1], over_y),
     ]
+    arrived(r1a, v_x1, xx)
+    part[slot(y, c, xx), :, lo] = add(slot(y, c, xx), lo, r1a[xx]).astype(bf16)
+    third[0].start()
+    arrived_hi(yy)
+    part[slot(yy, c, t_me), :, hi] = add(slot(yy, c, t_me), hi, r1b[yy]).astype(bf16)
+    third[1].start()
+    mine = slot(y, c, t_me)
+    arrived(r1a, v_x1, t_me)
+    arrived_hi(y)
     for d in third:
-        d.start()
-    mine = slot(y, c, t_me)
-    for d in third:
-        d.wait()
+        d.wait_recv()
     out_ref[:, lo] = (add(mine, lo, r1a[t_me]) + r2[0].astype(f32)).astype(bf16)
     out_ref[:, hi] = (add(mine, hi, r1b[y]) + r2[1].astype(f32)).astype(bf16)
-
-    for c in w_swaps + e_swaps + o_swaps + t_sends:
-        c.wait_send()
+    for d in first + second + third + t_passes:
+        d.wait_send()
+
+    for d in w_swaps + e_swaps + o_swaps + t_sends:
+        d.wait_send()
     for d in range(1, lines):
         pl.when(q + d < lines)(packet_to(d).wait_send)
 
@@ -580,23 +661,17 @@
     sp = heads * lines
     pad = 8
 
-    def by_head(tensor):
-        return tensor.reshape(tensor.shape[0], heads, key).transpose(1, 0, 2)
-
-    weights = jnp.concatenate(
-        [by_head(w) for w in (w_query, w_forget, w_input, w_outgate, w_bgate, w_cgate, w_value)],
-        axis=2,
-    )
-    outs = jnp.concatenate(
-        [out_rec.reshape(heads, key, span), out_conv.reshape(heads, key, span)], axis=1
-    )
+    weights = (w_query, w_forget, w_input, w_outgate, w_bgate, w_cgate, w_value)
     per = extra_decay.shape[0] // BLOCK
     extra = extra_decay.T.reshape(heads, per, BLOCK)
     extra = jnp.pad(extra, ((0, 0), (0, pad - per), (0, key - BLOCK)))
-    taps = jnp.pad(by_head(conv_taps), ((0, 0), (0, pad - conv_taps.shape[0]), (0, 0)))
     dma = pltpu.SemaphoreType.DMA
     half = model // 2
     scratch = [
+        pltpu.VMEM((rows, model), bf16),
+        pltpu.VMEM((heads, depth, 7 * key), bf16),
+        pltpu.VMEM((heads, 2 * key, span), bf16),
+        pltpu.VMEM((every, rows, model), bf16),
         pltpu.VMEM((every, rows, model), bf16),
         pltpu.VMEM((sp, depth, 7 * key), bf16),
         pltpu.VMEM((sp, 2 * key, span), bf16),
@@ -605,7 +680,6 @@
         pltpu.VMEM((length + pad, key), f32),
         pltpu.VMEM((length, key), f32),
         pltpu.VMEM((length, key), f32),
-        pltpu.VMEM((length, 2 * key), bf16),
         pltpu.VMEM((key + 2 * pad, key), f32),
         pltpu.VMEM((lines, key + 2 * pad, key), f32),
         pltpu.VMEM((key, key), f32),
@@ -618,18 +692,24 @@
         dma((sp,)), dma((sp,)), dma((sp,)), dma((sp,)),
         dma((sp,)), dma((sp,)), dma((heads,)), dma((every,)), dma((lines,)),
         dma((4,)), dma((4,)), dma((4,)), dma((4,)), dma((2,)), dma((2,)),
+        dma((heads,)), dma((2,)),
     ]
+    hbm = pl.BlockSpec(memory_space=pl.ANY)
+    vmem = pl.BlockSpec(memory_space=pltpu.VMEM)
     return pl.pallas_call(
         functools.partial(fused_kernel, heads, lines, groups, BLOCK),
         out_shape=jax.ShapeDtypeStruct((rows, model), bf16),
-        in_specs=[pl.BlockSpec(memory_space=pltpu.VMEM)] * 9,
+        in_specs=[hbm, vmem, (hbm,) * 7, hbm, hbm] + [vmem] * 5,
         out_specs=pl.BlockSpec(memory_space=pltpu.VMEM),
         scratch_shapes=scratch,
         compiler_params=pltpu.CompilerParams(
             collective_id=0, has_side_effects=True, vmem_limit_bytes=60 * 1024 * 1024
         ),
         name="mixer",
-    )(tokens, norm_gain[None], weights, outs, floor_gap, extra, start_state, state_gain[None], taps)
+    )(
+        tokens, norm_gain[None], weights, out_rec, out_conv, floor_gap, extra, start_state,
+        state_gain[None], conv_taps,
+    )
 
 
 def per_device(sp, tp, *args):

time: 151 us -> 121 us (0.80)
  Pallas kernels: 138 us -> 116 us
  local copies, waits for them, and re-layouts: 11.5 us -> 3.26 us
    pallas_call x1, Pallas kernels: 138 us -> 116 us  [fused(): pl.pallas_call(functools.partial(fused_kernel, heads, lines, groups, BLOC...]
    unnamed x36 -> x3, local copies, waits for them, and re-layouts: 9.28 us -> 2.57 us
where the time goes in v2:
time: 121 us; the launch traced here: 120 us
  Pallas kernels  116 us (96%)
  local copies, waits for them, and re-layouts  3.26 us (3%)
    pallas_call x1, Pallas kernels, fused(): pl.pallas_call(functools.partial(fused_kernel, heads, lines, groups, BLOC...  116 us
    unnamed x3, local copies, waits for them, and re-layouts  2.57 us

profile of v2, /device:TPU:24, one launch (start us, length us, event | category | flops | bytes accessed | tf_op | source)
XLA Modules:
  0.0 119.7 jit_solution(9684102870016858678)
XLA Ops:
  0.0 0.0 copy-start
  0.0 0.7 copy-done
  0.7 0.1 reshape.3
  0.8 0.6 pad.4.ed_ref
  1.4 116.4 %mixer.1 = bf16[128,2048]{1,0:T(8,128)(2,1)} custom-call(bf16[128,2048]{1,0:T(8,128)(2,1)} %tok_in.1, f32[1,2048]{1,0:T(1,128)} %bitcast.3, bf16[128,512]{1,0:T(8,128)(2,1)} %w_ins_0_.1, bf16[128,512]{1,0:T(8,128)(2,1)} %w_ins_1_.1, bf16[128,512]{1,0:T(8,128)(2,1)} %w_ins_2_.1, bf16[128,512]{1,0:T(8,128)(2,1)} %w_ins_3_.1, bf16[128,512]{1,0:T(8,128)(2,1)} %w_ins_4_.1, ...), custom_call_target="tpu_custom_call" | custom-call | tf_op jit(solution)/shard_map/mixer/pallas_call | solution.py:699
  117.8 1.9 %copy.18 = bf16[128,2048]{1,0:T(8,128)(2,1)} copy(bf16[128,2048]{1,0:T(8,128)(2,1)} %mixer.1) | data formatting | bytes 1048576
Async XLA Ops:
  0.0 0.7 copy-start

commit v3 on v2

--- a/solution.py
+++ b/solution.py
@@ -232,8 +232,8 @@
     ge,
     proj,
     gated,
-    mixed,
-    lifted,
+    runs,
+    befores,
     packet,
     packets,
     state,
@@ -503,36 +503,28 @@
     gap = gap_ref[pl.ds(r, 1), :]
     packet[...] = jnp.zeros_like(packet)
 
+    def writing(at):
+        return gap * sigmoid(-column(at, 1))
+
     def advance(b, _):
         at = pl.ds(pl.multiple_of(b * block, block), block)
-        query = column(at, 0)
-        query = query * sigmoid(query)
-        write = gap * sigmoid(-column(at, 1))
-        values = column(at, 2)
+        write = writing(at)
         extra = ge[b // per, pl.ds(lax.rem(b, per), 1), :]
         run = high_dot(tri, jnp.log1p(-write), ((1,), (0,))) + jnp.sum(
             wide * extra, axis=1, keepdims=True
         )
         final = run[block - 1 : block, :]
-        middle = 0.5 * final
-        scores = tri * high_dot(
-            query * jnp.exp(run - middle), write * jnp.exp(middle - run), ((1,), (1,))
-        )
-        before = packet[:key, :]
-        offset = packet[key : key + 1, :]
-        lift = query * jnp.exp(run)
-        mixed[at, :] = high_dot(scores, values, ((1,), (0,))) + high_dot(
-            lift, before, ((1,), (1,))
-        )
-        lifted[at, :] = lift * jnp.exp(offset)
-        packet[:key, :] = before * jnp.exp(final) + high_dot(
-            values, write * jnp.exp(final - run), ((0,), (0,))
-        )
-        packet[key : key + pad, :] = jnp.broadcast_to(offset + final, (pad, key))
+        runs[at, :] = run
+        before = packet[: key + pad, :]
+        befores[b] = before
+        packet[:key, :] = before[:key] * jnp.exp(final) + high_dot(
+            column(at, 2), write * jnp.exp(final - run), ((0,), (0,))
+        )
+        packet[key : key + pad, :] = before[key:] + final
         gated[pl.ds(pl.multiple_of(b * block + pad, pad), block), :] = column(at, 5) * column(at, 6)
         return 0
 
-    lax.fori_loop(0, blocks, advance, 0)
+    lax.fori_loop(0, blocks, advance, 0, unroll=4)
     packet[key + pad : key + 2 * pad, :] = gated[length : length + pad, :]
 
     def packet_to(d):
@@ -565,7 +557,23 @@
     def finish(e):
         start = pl.multiple_of(e * rows, rows)
         at = pl.ds(start, rows)
-        m = mixed[at, :] + high_dot(lifted[at, :], state[...], ((1,), (1,)))
+        mixed = []
+        for u in range(rows // block):
+            here = pl.ds(pl.multiple_of(start + u * block, block), block)
+            query = column(here, 0)
+            query = query * sigmoid(query)
+            run = runs[here, :]
+            middle = 0.5 * run[block - 1 : block, :]
+            scores = tri * high_dot(
+                query * jnp.exp(run - middle), writing(here) * jnp.exp(middle - run), ((1,), (1,))
+            )
+            before = befores[e * (rows // block) + u]
+            whole = before[:key] + state[...] * jnp.exp(before[key : key + 1])
+            mixed.append(
+                high_dot(scores, column(here, 2), ((1,), (0,)))
+                + high_dot(query * jnp.exp(run), whole, ((1,), (1,)))
+            )
+        m = jnp.concatenate(mixed, axis=0)
         gate = column(at, 3)
         rec = m * rms_scale(m) * sgain_ref[...] * (gate * sigmoid(gate))
         near = gated[pl.ds(start, rows + pad), :]
@@ -586,11 +594,6 @@
     lo, hi = pl.ds(0, half), pl.ds(half, half)
     order = ((yy, xx), (yy, t_me), (y, xx), (y, t_me))
     first = []
-    for a, b in order:
-        n = 2 * a + b
-        finish(slot(a, cc, b))
-        first.append(copy(part.at[slot(a, cc, b)], r0.at[n], s_x0.at[n], v_x0.at[n], core))
-        first[-1].start()
 
     def add(e, cols, other):
         return part[e, :, cols].astype(f32) + other.astype(f32)
@@ -608,8 +611,12 @@
 
     second = [to_y(xx), to_x(yy), to_y(t_me), to_x(y)]
     sends = [second[:2], second[2:3], second[3:], []]
-    for (a, b), ready, d in zip(order, sends, first):
-        e = slot(a, c, b)
+    for (a, b), ready in zip(order, sends):
+        e, n = slot(a, c, b), 2 * a + b
+        finish(slot(a, cc, b))
+        d = copy(part.at[slot(a, cc, b)], r0.at[n], s_x0.at[n], v_x0.at[n], core)
+        d.start()
+        first.append(d)
         finish(e)
         d.wait_recv()
         part[e] = (part[e].astype(f32) + r0[2 * a + b].astype(f32)).astype(bf16)
@@ -679,7 +686,7 @@
         pltpu.VMEM((length, 7 * key), bf16),
         pltpu.VMEM((length + pad, key), f32),
         pltpu.VMEM((length, key), f32),
-        pltpu.VMEM((length, key), f32),
+        pltpu.VMEM((length // BLOCK, key + pad, key), f32),
         pltpu.VMEM((key + 2 * pad, key), f32),
         pltpu.VMEM((lines, key + 2 * pad, key), f32),
         pltpu.VMEM((key, key), f32),

time: 121 us -> 114 us (0.942)
  Pallas kernels: 116 us -> 110 us
    pallas_call x1, Pallas kernels: 116 us -> 110 us  [fused(): pl.pallas_call(functools.partial(fused_kernel, heads, lines, groups, BLOC...]
where the time goes in v3:
time: 114 us
  Pallas kernels  110 us (96%)
  local copies, waits for them, and re-layouts  3.26 us (3%)
    pallas_call x1, Pallas kernels, fused(): pl.pallas_call(functools.partial(fused_kernel, heads, lines, groups, BLOC...  110 us
    unnamed x3, local copies, waits for them, and re-layouts  2.57 us

profile of v3, /device:TPU:24, one launch (start us, length us, event | category | flops | bytes accessed | tf_op | source)
XLA Modules:
  0.0 113.7 jit_solution(4824582580620737197)
XLA Ops:
  0.0 0.0 copy-start
  0.0 0.7 copy-done
  0.7 0.1 reshape.3
  0.8 0.6 pad.4.ed_ref
  1.4 110.4 %mixer.1 = bf16[128,2048]{1,0:T(8,128)(2,1)} custom-call(bf16[128,2048]{1,0:T(8,128)(2,1)} %tok_in.1, f32[1,2048]{1,0:T(1,128)} %bitcast.3, bf16[128,512]{1,0:T(8,128)(2,1)} %w_ins_0_.1, bf16[128,512]{1,0:T(8,128)(2,1)} %w_ins_1_.1, bf16[128,512]{1,0:T(8,128)(2,1)} %w_ins_2_.1, bf16[128,512]{1,0:T(8,128)(2,1)} %w_ins_3_.1, bf16[128,512]{1,0:T(8,128)(2,1)} %w_ins_4_.1, ...), custom_call_target="tpu_custom_call" | custom-call | tf_op jit(solution)/shard_map/mixer/pallas_call | solution.py:706
  111.8 1.9 %copy.18 = bf16[128,2048]{1,0:T(8,128)(2,1)} copy(bf16[128,2048]{1,0:T(8,128)(2,1)} %mixer.1) | data formatting | bytes 1048576
Async XLA Ops:
  0.0 0.7 copy-start
